TPU v7x, 32 devices: a whole 2x2x4 slice. The times are simulated.
32 devices in a mesh: sp: 8 (over z, y), tp: 4 (over x, core).
Axes of the slice: x: 2, y: 2, z: 4, core: 2. Of those that a mesh axis runs over, the one named last changes fastest.
Arguments:
- queries: bfloat16 [8192, 1024], P('sp', 'tp'), may hold values from -6 to 6
- keys: bfloat16 [8192, 1024], P('sp', 'tp'), may hold values from -6 to 6
- values: bfloat16 [8192, 1024], P('sp', 'tp'), may hold values from -6 to 6
- gates: bfloat16 [8192, 1024], P('sp', 'tp'), may hold values from -6 to 6
- log_decay: float32 [8192, 8], P('sp', 'tp'), may hold values from -1.6 to 0, as said below
- norm_gain: float32 [8, 128], P('tp'), may hold values from 0.1 to 1.9
- out_weight: bfloat16 [1024, 2048], P('tp'), may hold values from -0.1875 to 0.1875
- resid: bfloat16 [8192, 2048], P(('sp', 'tp')), may hold values from -6 to 6
- post_mix_gain: float32 [2048], replicated, may hold values from 0.1 to 1.9
- pre_ffn_gain: float32 [2048], replicated, may hold values from 0.1 to 1.9
- w_gate: bfloat16 [2048, 5632], P('sp', 'tp'), may hold values from -0.125 to 0.125
- w_up: bfloat16 [2048, 5632], P('sp', 'tp'), may hold values from -0.125 to 0.125
- w_down: bfloat16 [5632, 2048], P('tp', 'sp'), may hold values from -0.078125 to 0.078125
- post_ffn_gain: float32 [2048], replicated, may hold values from 0.1 to 1.9
Outputs:
- updated: bfloat16 [8192, 2048], P(('sp', 'tp'))
Inputs may be any that keep to these rules, and one draw needn't show every extreme that they name: `log_decay`: every entry is negative.
All inputs are finite; a program needn't handle non-finite values.
Results may differ from a plain program's by a relative error of at most 0.02.
Values may be sent and summed in bfloat16 or wider, within the bound.
A program may use at most 128 MiB of HBM per device.

v0:
```python
import jax
import jax.numpy as jnp
from jax import lax
from jax.sharding import PartitionSpec as P

BLOCK = 512
EPSILON = 1e-06


def entering(x, axis, join, neutral):
    place = lax.axis_index(axis)
    gathered = jax.tree.map(
        lambda a, kind: lax.all_gather(a.astype(kind), axis), x, (jnp.bfloat16, jnp.bfloat16)
    )
    state = jax.tree.map(lambda a, e: jnp.zeros_like(a) + jnp.asarray(e, a.dtype), x, neutral)

    def one(step, state):
        return join(
            state,
            jax.tree.map(
                lambda a, own: lax.dynamic_index_in_dim(a, step, 0, False).astype(own.dtype),
                gathered,
                x,
            ),
        )

    return lax.fori_loop(0, place, one, state)


def rms_norm(values_in, gain_vec):
    widened = values_in.astype(jnp.float32)
    return (
        widened
        * lax.rsqrt(jnp.mean(widened * widened, axis=-1, keepdims=True) + EPSILON)
        * gain_vec
    )


def block_step(carried, pieces):
    query_blk, key_blk, value_blk, decay_blk = pieces
    length = query_blk.shape[1]
    key_scale = query_blk.shape[2] ** (-0.5)
    cumulative = jnp.cumsum(decay_blk, axis=1)
    log_gap = cumulative[:, :, None] - cumulative[:, None, :]
    causal = lax.broadcasted_iota(jnp.int32, (length, length), 0) >= lax.broadcasted_iota(
        jnp.int32, (length, length), 1
    )
    weight = jnp.where(causal[None], jnp.exp(jnp.minimum(log_gap, 0.0)), 0.0)
    products = jnp.einsum("htd,hsd->hts", query_blk, key_blk, preferred_element_type=jnp.float32)
    scores = (products * key_scale * weight).astype(jnp.bfloat16)
    within = jnp.einsum("hts,hsd->htd", scores, value_blk, preferred_element_type=jnp.float32)
    carried_term = (
        jnp.einsum(
            "htd,hde->hte", query_blk.astype(jnp.float32), carried, precision=lax.Precision.HIGHEST
        )
        * jnp.exp(cumulative)[:, :, None]
    )
    to_end = jnp.exp(cumulative[:, -1:] - cumulative) * key_scale
    scaled_keys = (key_blk.astype(jnp.float32) * to_end[:, :, None]).astype(jnp.bfloat16)
    added = jnp.einsum("hsd,hse->hde", scaled_keys, value_blk, preferred_element_type=jnp.float32)
    carried = jnp.exp(cumulative[:, -1])[:, None, None] * carried + added
    return (carried, within + carried_term)


def to_blocks(matrix, block_len, head_count):
    row_count = matrix.shape[0]
    return matrix.reshape(row_count // block_len, block_len, head_count, -1).transpose(0, 2, 1, 3)


def finish_heads(retention, gates, norm_gain):
    centered = retention - jnp.mean(retention, axis=-1, keepdims=True)
    variance = jnp.mean(centered * centered, axis=-1, keepdims=True)
    normed = centered * lax.rsqrt(variance + EPSILON) * norm_gain[None]
    gate_vals = gates.astype(jnp.float32).reshape(normed.shape)
    return (jax.nn.silu(gate_vals) * normed).reshape(normed.shape[0], -1).astype(jnp.bfloat16)


def combine_states(earlier, later):
    return (earlier[0] * later[0], later[0][:, None, None] * earlier[1] + later[1])


def per_device(
    queries,
    keys,
    values,
    gates,
    log_decay,
    norm_gain,
    out_weight,
    resid,
    post_mix_gain,
    pre_ffn_gain,
    w_gate,
    w_up,
    w_down,
    post_ffn_gain,
):
    row_count = queries.shape[0]
    head_count = log_decay.shape[1]
    head_dim = queries.shape[1] // head_count
    block_count = row_count // BLOCK
    query_blocks = to_blocks(queries, BLOCK, head_count)
    key_blocks = to_blocks(keys, BLOCK, head_count)
    value_blocks = to_blocks(values, BLOCK, head_count)
    decay_blocks = log_decay.reshape(block_count, BLOCK, head_count).transpose(0, 2, 1)
    start_state = jnp.zeros((head_count, head_dim, head_dim), jnp.float32)
    local_state, outputs = lax.scan(
        block_step, start_state, (query_blocks, key_blocks, value_blocks, decay_blocks)
    )
    retention = outputs.transpose(0, 2, 1, 3).reshape(row_count, head_count, head_dim)
    cumulative = jnp.cumsum(log_decay, axis=0)
    local_decay = jnp.exp(cumulative[-1])
    identity = (jnp.ones_like(local_decay), jnp.zeros_like(local_state))
    incoming = entering((local_decay, local_state), "sp", combine_states, identity)
    query_rows = queries.reshape(row_count, head_count, head_dim).astype(jnp.float32)
    retention = (
        retention
        + jnp.einsum("thd,hde->the", query_rows, incoming[1], precision=lax.Precision.HIGHEST)
        * jnp.exp(cumulative)[:, :, None]
    )
    retained = finish_heads(retention, gates, norm_gain)
    quarter = resid.shape[0]
    regrouped = lax.all_to_all(retained, "tp", split_axis=0, concat_axis=1, tiled=True)
    group_rows = out_weight.shape[0]
    empty_mix = jnp.zeros((quarter, out_weight.shape[1]), jnp.float32)
    running = empty_mix
    shard_piece = lax.all_gather(out_weight, "tp", axis=0, tiled=True)
    for offset in range(shard_piece.shape[0] // group_rows):
        columns = lax.dynamic_slice_in_dim(regrouped, offset * group_rows, group_rows, 1)
        part = jnp.dot(
            columns,
            shard_piece[offset * group_rows : (offset + 1) * group_rows],
            preferred_element_type=jnp.float32,
        )
        running = running + part.astype(jnp.bfloat16).astype(jnp.float32)
    mixed = running
    mixed = mixed.astype(jnp.bfloat16)
    middle = (resid.astype(jnp.float32) + rms_norm(mixed, post_mix_gain)).astype(jnp.bfloat16)
    ffn_input = rms_norm(middle, pre_ffn_gain).astype(jnp.bfloat16)
    gathered = lax.all_gather(ffn_input, "tp", axis=0, tiled=True)
    columns = gathered
    gate_act = jnp.dot(
        columns,
        lax.all_gather(w_gate, "sp", axis=0, tiled=True),
        preferred_element_type=jnp.float32,
    )
    up_act = jnp.dot(
        columns, lax.all_gather(w_up, "sp", axis=0, tiled=True), preferred_element_type=jnp.float32
    )
    down_full = lax.all_gather(w_down, "sp", axis=1, tiled=True)
    hidden = (jax.nn.silu(gate_act) * up_act).astype(jnp.bfloat16)
    branch = lax.psum_scatter(
        jnp.dot(hidden, down_full, preferred_element_type=jnp.float32)
        .astype(jnp.bfloat16)
        .astype(jnp.float32)
        .astype(jnp.bfloat16),
        "tp",
        scatter_dimension=0,
        tiled=True,
    )
    return (middle.astype(jnp.float32) + rms_norm(branch, post_ffn_gain)).astype(jnp.bfloat16)


def solution(mesh):
    in_specs = (
        P("sp", "tp"),
        P("sp", "tp"),
        P("sp", "tp"),
        P("sp", "tp"),
        P("sp", "tp"),
        P("tp", None),
        P("tp", None),
        P(("sp", "tp"), None),
        P(),
        P(),
        P("sp", "tp"),
        P("sp", "tp"),
        P("tp", "sp"),
        P(),
    )
    out_specs = P(("sp", "tp"), None)
    return jax.shard_map(
        per_device, mesh=mesh, in_specs=in_specs, out_specs=out_specs, check_vma=False
    )
```

profile of v0, /device:TPU:0, one launch (start us, length us, event | category | flops | bytes accessed | tf_op | source)
XLA Modules:
  0.0 438.4 jit_solution(6785753459974340258)
XLA Ops:
  6.5 0.7 all-gather.8.cloned.1.call-update
  7.3 0.7 all-gather.12.cloned.1.call-update
  8.1 0.7 copy.104
  8.8 0.6 reduce-window.16
  9.5 0.2 reduce-window.17
  9.8 0.2 fusion.48
  10.0 22.3 %all-gather.1 = bf16[8,1,2]{2,1,0:T(2,128)(2,1)S(1)} all-gather(bf16[1,1,2]{2,1,0:T(2,128)(2,1)S(1)} %bitcast.154), channel_id=1, replica_groups=mesh['sp'=8,'tp'=4] {'sp'}, dimensions={0}, use_global_device_ids=true | all-gather | bytes 36 | tf_op jit(solution)/shard_map/all_gather | solution.py:13
  32.8 9.6 %while.26 = (s32[]{:T(128)}, f32[2,128,128]{2,1,0:T(8,128)S(1)}, f32[2,2,512,128]{3,2,1,0:T(8,128)}, f32[2,2,512]{2,1,0:T(2,128)S(1)}, bf16[2,2,512,128]{3,1,2,0...) while((s32[]{:T(128)}, f32[2,128,128]{2,1,0:T(8,128)S(1)}, ...), condition=%wide.region_3.4_spmd.clone, body=%wide.region_0.3_spmd.clone.sunk | while | flops 507643936 | bytes 5702508 | solution.py:107
  32.8 0.6 reduce-window.26
  33.6 0.2 reduce-window.27
  33.9 0.4 constant_dynamic-slice_fusion.12
  34.3 0.2 constant_dynamic-slice_fusion.11
  34.5 1.0 fusion.75
  35.8 1.2 fusion.76
  37.0 0.5 convolution_add_fusion.2
  37.6 0.6 reduce-window.26
  38.7 0.4 constant_dynamic-slice_fusion.12
  39.0 0.2 constant_dynamic-slice_fusion.11
  39.3 1.0 fusion.75
  40.6 1.2 fusion.76
  41.8 0.5 convolution_add_fusion.2
  42.4 1.6 copy.57
  44.1 0.9 reshape.175
  45.0 0.2 copy.53
  45.2 33.1 %all-gather = bf16[16,128,128]{2,1,0:T(8,128)(2,1)S(1)} all-gather(bf16[2,128,128]{2,1,0:T(8,128)(2,1)S(1)} %convert_element_type.103), channel_id=2, replica_groups=mesh['sp'=8,'tp'=4] {'sp'}, dimensions={0}, use_global_device_ids=true | all-gather | bytes 589824 | tf_op jit(solution)/shard_map/all_gather | solution.py:13
  78.4 0.7 fusion.51
  79.3 0.4 multiply_convert_fusion.4
  79.7 0.4 convert_element_type.105
  80.1 11.4 %all_to_all.16 = bf16[4,256,256]{1,2,0:T(8,128)(2,1)S(1)} all-to-all(bf16[4,256,256]{1,2,0:T(8,128)(2,1)S(1)} %copy.62), channel_id=1, replica_groups=mesh['sp'=8,'tp'=4] {'tp'}, dimensions={0} | all-to-all | bytes 1048576 | tf_op jit(solution)/shard_map/all_to_all | solution.py:123
  91.5 1.8 fusion.22
  93.4 1.7 fusion.23
  95.1 0.5 fusion.24
  95.6 0.8 fusion.25
  96.4 0.4 copy-done.3
  96.8 0.6 fusion.31
  97.4 1.3 fusion.33
  98.8 0.5 all-gather.14.cloned.1.call-update
  99.4 0.5 all-gather.16.cloned.1.call-update
  99.9 0.2 reduce-scatter.2.cloned.1.call-start
  100.1 41.9 %all-gather.12.cloned.1.call-done = bf16[2048,1408]{1,0:T(8,128)(2,1)} async-done(((bf16[256,1408]{1,0:T(8,128)(2,1)}), bf16[2048,1408]{1,0:T(8,128)(2,1)}) %all-gather.12.cloned.1.call-update) | async-done | bytes 5767184 | tf_op jit(solution)/shard_map/all_gather | solution.py:144
  142.0 34.2 %all-gather.10.cloned.1.call-done = bf16[1024,2048]{1,0:T(8,128)(2,1)} async-done(((bf16[256,2048]{1,0:T(8,128)(2,1)}), bf16[1024,2048]{1,0:T(8,128)(2,1)}) %all-gather.10.cloned.1.call-update) | async-done | bytes 4194320 | tf_op jit(solution)/shard_map/all_gather | solution.py:140
  176.3 11.7 %fusion.52 = f32[1024,1408]{1,0:T(8,128)} fusion(bf16[1024,2048]{1,0:T(8,128)(2,1)} %all-gather.10.cloned.1.call-done, bf16[2048,1408]{1,0:T(8,128)(2,1)} %all-gather.12.cloned.1.call-done), kind=kOutput, calls=%fused_computation.97 | convolution fusion | flops 5905580032 | bytes 15728640 | tf_op jit(solution)/shard_map/dot_general | solution.py:142
  188.0 82.7 %all-gather.14.cloned.1.call-done = bf16[2048,1408]{1,0:T(8,128)(2,1)} async-done(((bf16[256,1408]{1,0:T(8,128)(2,1)}), bf16[2048,1408]{1,0:T(8,128)(2,1)}) %all-gather.14.cloned.1.call-update) | async-done | bytes 5767184 | tf_op jit(solution)/shard_map/all_gather | solution.py:148
  270.7 93.2 %all-gather.16.cloned.1.call-done = bf16[1408,2048]{1,0:T(8,128)(2,1)} async-done(((bf16[1408,256]{1,0:T(8,128)(2,1)}), bf16[1408,2048]{1,0:T(8,128)(2,1)}) %all-gather.16.cloned.1.call-update) | async-done | bytes 5767184 | tf_op jit(solution)/shard_map/all_gather | solution.py:150
  363.9 20.5 %convolution_convert_fusion = bf16[1024,2048]{1,0:T(8,128)(2,1)} fusion(bf16[1408,2048]{1,0:T(8,128)(2,1)} %all-gather.16.cloned.1.call-done, f32[1024,1408]{1,0:T(8,128)} %fusion.52, bf16[1024,2048]{1,0:T(8,128)(2,1)} %all-gather.10.cloned.1.call-done, bf16[2048,1408]{1,0:T(8,128)(2,1)} %all-gather.14.cloned.1.call-done), kind=kOutput, calls=%fused_computation.38 | convolution fusion | flops 11821907968 | bytes 25690112 | tf_op jit(solution)/shard_map/dot_general | solution.py:153
  384.5 42.9 %reduce-scatter.2.cloned.1.call-done = bf16[256,2048]{1,0:T(8,128)(2,1)} async-done(((bf16[1024,2048]{1,0:T(8,128)(2,1)}), bf16[256,2048]{1,0:T(8,128)(2,1)}) %reduce-scatter.2.cloned.1.call-update) | async-done | bytes 1048592 | tf_op jit(solution)/shard_map/reduce_scatter | solution.py:152
  427.4 1.5 fusion.29
  428.9 2.6 fusion.34
  (72 shorter events, 2.6 us)
Async XLA Ops:
  6.5 25.8 %copy-start.5 = (bf16[1024,256]{1,0:T(8,128)(2,1)S(1)}, bf16[1024,256]{1,0:T(8,128)(2,1)}, u32[]{:S(2)}) copy-start(bf16[1024,256]{1,0:T(8,128)(2,1)} %param.19) | copy-start | bytes 1572868
  6.5 26.0 %copy-start.6 = (bf16[1024,256]{1,0:T(8,128)(2,1)S(1)}, bf16[1024,256]{1,0:T(8,128)(2,1)}, u32[]{:S(2)}) copy-start(bf16[1024,256]{1,0:T(8,128)(2,1)} %param.20) | copy-start | bytes 1572868
  6.5 26.1 %copy-start.1 = (bf16[1024,256]{1,0:T(8,128)(2,1)S(1)}, bf16[1024,256]{1,0:T(8,128)(2,1)}, u32[]{:S(2)}) copy-start(bf16[1024,256]{1,0:T(8,128)(2,1)} %param.18) | copy-start | bytes 1572868
  6.5 85.0 %all-gather.8.cloned.1.call-start = ((), (), s32[]{:S(2)}) async-start(), calls=%async_computation.2 | async-start | bytes 5242880 | tf_op jit(solution)/shard_map/all_gather | solution.py:127
  7.3 25.5 %copy-start.7 = (f32[1024,2]{0,1:T(2,128)S(1)}, f32[1024,2]{0,1:T(2,128)}, u32[]{:S(2)}) copy-start(f32[1024,2]{0,1:T(2,128)} %param.22) | copy-start | bytes 24580
  7.3 134.8 %all-gather.12.cloned.1.call-start = ((), (), s32[]{:S(2)}) async-start(), calls=%async_computation.4 | async-start | bytes 6488064 | tf_op jit(solution)/shard_map/all_gather | solution.py:144
  8.0 168.3 %all-gather.10.cloned.1.call-start = ((), (), s32[]{:S(2)}) async-start(), calls=%async_computation.3 | async-start | bytes 5242880 | tf_op jit(solution)/shard_map/all_gather | solution.py:140
  42.4 2.6 copy-start.4
  45.0 33.4 %copy-start.2 = (bf16[1024,256]{1,0:T(8,128)(2,1)S(1)}, bf16[1024,256]{1,0:T(8,128)(2,1)}, u32[]{:S(2)}) copy-start(bf16[1024,256]{1,0:T(8,128)(2,1)} %param.18) | copy-start | bytes 1572868
  78.3 0.9 copy-start.11
  91.5 3.5 copy-start
  95.5 1.2 copy-start.3
  95.5 1.2 copy-start.8
  96.4 1.1 copy-start.9
  98.7 171.9 %all-gather.14.cloned.1.call-start = ((), (), s32[]{:S(2)}) async-start(), calls=%async_computation.5 | async-start | bytes 6488064 | tf_op jit(solution)/shard_map/all_gather | solution.py:148
  99.3 264.6 %all-gather.16.cloned.1.call-start = ((), (), s32[]{:S(2)}) async-start(), calls=%async_computation.6 | async-start | bytes 6488064 | tf_op jit(solution)/shard_map/all_gather | solution.py:150
  99.9 327.5 %reduce-scatter.2.cloned.1.call-start = ((), (), s32[]{:S(2)}) async-start(), calls=%async_computation.7 | async-start | bytes 5242880 | tf_op jit(solution)/shard_map/reduce_scatter | solution.py:152
  384.4 44.5 %copy-start.10 = (f32[2048]{0:T(1024)S(1)}, f32[2048]{0:T(1024)}, u32[]{:S(2)}) copy-start(f32[2048]{0:T(1024)} %param.31) | copy-start | bytes 24580
Sparse Core Ops, SparseCore 0:
  8.9 37.1 all-gather.7
  48.3 93.7 all-gather.11
  143.6 32.6 all-gather.9
  178.3 92.3 all-gather.13
  272.6 91.2 all-gather.15
  384.6 42.7 reduce-scatter.1
where the time goes:
time: 439 us; the launch traced here: 438 us
  waiting for transfers between devices  297 us (68%)
  blocking collectives  66.8 us (15%)
  matrix products  43.3 us (10%)
  between operations  13.8 us (3%)
  other arithmetic  9.76 us (2%)
  local copies, waits for them, and re-layouts  6.82 us (2%)
    all_gather x1, waiting for transfers between devices, per_device(): down_full = lax.all_gather(w_down, 'sp', axis=1, tiled=True)  93.2 us
    all_gather x1, waiting for transfers between devices, per_device(): lax.all_gather(w_up, 'sp', axis=0, tiled=True)  82.7 us
    all_gather x2, blocking collectives, entering(): lax.all_gather(a.astype(kind), axis)  55.4 us
    reduce_scatter x1, waiting for transfers between devices, per_device(): lax.psum_scatter(jnp.dot(hidden, down_full, preferred_element_type=jnp.fl...  42.9 us
    all_gather x1, waiting for transfers between devices, per_device(): lax.all_gather(w_gate, 'sp', axis=0, tiled=True)  41.9 us
    all_gather x1, waiting for transfers between devices, per_device(): gathered = lax.all_gather(ffn_input, 'tp', axis=0, tiled=True)  34.2 us
    dot_general x1, matrix products, per_device(): jnp.dot(hidden, down_full, preferred_element_type=jnp.float32)  20.5 us
    dot_general x1, matrix products, per_device(): jnp.dot(columns, lax.all_gather(w_gate, 'sp', axis=0, tiled=True), prefer...  11.7 us
  transfers between devices with their start and end apart: 6, of which 5 were waited for; matrix products, arithmetic and copies ran while one was open for 8% of the time, Pallas kernels for 0%

commit v1 on v0

--- a/solution.py
+++ b/solution.py
@@ -145,7 +145,11 @@
         preferred_element_type=jnp.float32,
     )
     up_act = jnp.dot(
-        columns, lax.all_gather(w_up, "sp", axis=0, tiled=True), preferred_element_type=jnp.float32
+        columns,
+        jnp.concatenate(
+            lax.all_to_all(jnp.stack([w_up] * lax.axis_size("sp")), "sp", 0, 0), axis=0
+        ),
+        preferred_element_type=jnp.float32,
     )
     down_full = lax.all_gather(w_down, "sp", axis=1, tiled=True)
     hidden = (jax.nn.silu(gate_act) * up_act).astype(jnp.bfloat16)

time: 439 us -> 418 us (0.952)
  waiting for transfers between devices: 297 us -> 269 us
  starting transfers between devices: 0.38 us -> 5.04 us
    all_gather x1 -> x0, waiting for transfers between devices: 82.7 us -> none  [per_device(): lax.all_gather(w_up, 'sp', axis=0, tiled=True)]
    all_gather x1, waiting for transfers between devices: 41.9 us -> 77.9 us  [per_device(): lax.all_gather(w_gate, 'sp', axis=0, tiled=True)]
    all_gather x1, waiting for transfers between devices: 34.2 us -> 63.2 us  [per_device(): gathered = lax.all_gather(ffn_input, 'tp', axis=0, tiled=True)]
    all_gather x1, waiting for transfers between devices: 93.2 us -> 76.3 us  [per_device(): down_full = lax.all_gather(w_down, 'sp', axis=1, tiled=True)]
    all_to_all x0 -> x1, waiting for transfers between devices: none -> 7.07 us  [per_device(): lax.all_to_all(jnp.stack([w_up] * lax.axis_size('sp')), 'sp', 0, 0)]
    all_to_all x0 -> x1, starting transfers between devices: none -> 4.7 us  [per_device(): lax.all_to_all(jnp.stack([w_up] * lax.axis_size('sp')), 'sp', 0, 0)]
  transfers between devices with their start and end apart: 6 -> 6, of which waited for: 5 -> 5; matrix products, arithmetic and copies ran while one was open for 8% -> 9% of each run, Pallas kernels for 0% -> 0%
where the time goes in v1:
time: 418 us; the launch traced here: 417 us
  waiting for transfers between devices  269 us (64%)
  blocking collectives  66.8 us (16%)
  matrix products  43.2 us (10%)
  between operations  13.5 us (3%)
  local copies, waits for them, and re-layouts  9.79 us (2%)
  other arithmetic  9.75 us (2%)
  starting transfers between devices  5.04 us (1%)
    all_gather x1, waiting for transfers between devices, per_device(): lax.all_gather(w_gate, 'sp', axis=0, tiled=True)  77.9 us
    all_gather x1, waiting for transfers between devices, per_device(): down_full = lax.all_gather(w_down, 'sp', axis=1, tiled=True)  76.3 us
    all_gather x1, waiting for transfers between devices, per_device(): gathered = lax.all_gather(ffn_input, 'tp', axis=0, tiled=True)  63.2 us
    all_gather x2, blocking collectives, entering(): lax.all_gather(a.astype(kind), axis)  55.4 us
    reduce_scatter x1, waiting for transfers between devices, per_device(): lax.psum_scatter(jnp.dot(hidden, down_full, preferred_element_type=jnp.fl...  42.9 us
    dot_general x1, matrix products, per_device(): jnp.dot(hidden, down_full, preferred_element_type=jnp.float32)  20.5 us
    dot_general x1, matrix products, per_device(): jnp.dot(columns, lax.all_gather(w_gate, 'sp', axis=0, tiled=True), prefer...  11.7 us
    all_to_all x1, blocking collectives, per_device(): lax.all_to_all(retained, 'tp', split_axis=0, concat_axis=1, tiled=True)  11.4 us
  transfers between devices with their start and end apart: 6, of which 5 were waited for; matrix products, arithmetic and copies ran while one was open for 9% of the time, Pallas kernels for 0%

profile of v1, /device:TPU:0, one launch (start us, length us, event | category | flops | bytes accessed | tf_op | source)
XLA Modules:
  0.0 417.5 jit_solution(11709244750776716072)
XLA Ops:
  6.5 0.7 all-gather.7.cloned.1.call-update
  7.3 0.7 all-gather.11.cloned.1.call-update
  8.1 0.7 copy.104
  8.8 0.6 reduce-window.16
  9.5 0.2 reduce-window.17
  9.8 0.2 fusion.48
  10.0 22.3 %all-gather.1 = bf16[8,1,2]{2,1,0:T(2,128)(2,1)S(1)} all-gather(bf16[1,1,2]{2,1,0:T(2,128)(2,1)S(1)} %bitcast.155), channel_id=1, replica_groups=mesh['sp'=8,'tp'=4] {'sp'}, dimensions={0}, use_global_device_ids=true | all-gather | bytes 36 | tf_op jit(solution)/shard_map/all_gather | solution.py:13
  32.8 9.5 %while.26 = (s32[]{:T(128)}, f32[2,128,128]{2,1,0:T(8,128)S(1)}, f32[2,2,512,128]{3,2,1,0:T(8,128)}, f32[2,2,512]{2,1,0:T(2,128)S(1)}, bf16[2,2,512,128]{3,1,2,0...) while((s32[]{:T(128)}, f32[2,128,128]{2,1,0:T(8,128)S(1)}, ...), condition=%wide.region_3.4_spmd.clone, body=%wide.region_0.3_spmd.clone.sunk | while | flops 507643936 | bytes 5702508 | solution.py:107
  32.8 0.6 reduce-window.26
  33.9 0.4 constant_dynamic-slice_fusion.12
  34.2 0.2 constant_dynamic-slice_fusion.11
  34.5 1.0 fusion.75
  35.8 1.2 fusion.76
  37.0 0.5 convolution_add_fusion.2
  37.6 0.6 reduce-window.26
  38.6 0.4 constant_dynamic-slice_fusion.12
  39.0 0.2 constant_dynamic-slice_fusion.11
  39.3 1.0 fusion.75
  40.6 1.2 fusion.76
  41.7 0.5 convolution_add_fusion.2
  42.3 1.7 copy.57
  44.0 0.9 reshape.180
  44.9 0.2 copy.53
  45.1 33.1 %all-gather = bf16[16,128,128]{2,1,0:T(8,128)(2,1)S(1)} all-gather(bf16[2,128,128]{2,1,0:T(8,128)(2,1)S(1)} %convert_element_type.103), channel_id=2, replica_groups=mesh['sp'=8,'tp'=4] {'sp'}, dimensions={0}, use_global_device_ids=true | all-gather | bytes 589824 | tf_op jit(solution)/shard_map/all_gather | solution.py:13
  78.3 0.7 fusion.51
  79.2 0.4 multiply_convert_fusion.4
  79.6 0.4 convert_element_type.105
  80.0 11.4 %all_to_all.21 = bf16[4,256,256]{1,2,0:T(8,128)(2,1)S(1)} all-to-all(bf16[4,256,256]{1,2,0:T(8,128)(2,1)S(1)} %copy.62), channel_id=1, replica_groups=mesh['sp'=8,'tp'=4] {'tp'}, dimensions={0} | all-to-all | bytes 1048576 | tf_op jit(solution)/shard_map/all_to_all | solution.py:123
  91.4 1.8 fusion.22
  93.3 1.7 fusion.23
  95.0 0.5 fusion.24
  95.5 0.8 fusion.25
  96.3 0.4 copy-done.3
  96.7 0.6 fusion.31
  97.3 1.3 fusion.33
  98.7 2.9 stack.2
  101.6 4.7 %all-to-all-start.1 = ((bf16[8,256,1408]{2,1,0:T(8,128)(2,1)}), bf16[8,256,1408]{2,1,0:T(8,128)(2,1)}, u32[]{:S(2)}, u32[]{:S(2)}) async-start(bf16[8,256,1408]{2,1,0:T(8,128)(2,1)} %stack.2), calls=%async_computation.1 | async-start | bytes 11534336 | tf_op jit(solution)/shard_map/all_to_all | solution.py:150
  106.4 0.5 all-gather.13.cloned.1.call-update
  106.9 0.2 reduce-scatter.2.cloned.1.call-start
  107.1 77.9 %all-gather.11.cloned.1.call-done = bf16[2048,1408]{1,0:T(8,128)(2,1)} async-done(((bf16[256,1408]{1,0:T(8,128)(2,1)}), bf16[2048,1408]{1,0:T(8,128)(2,1)}) %all-gather.11.cloned.1.call-update) | async-done | bytes 5767184 | tf_op jit(solution)/shard_map/all_gather | solution.py:144
  185.0 63.2 %all-gather.9.cloned.1.call-done = bf16[1024,2048]{1,0:T(8,128)(2,1)} async-done(((bf16[256,2048]{1,0:T(8,128)(2,1)}), bf16[1024,2048]{1,0:T(8,128)(2,1)}) %all-gather.9.cloned.1.call-update) | async-done | bytes 4194320 | tf_op jit(solution)/shard_map/all_gather | solution.py:140
  248.2 11.7 %fusion.52 = f32[1024,1408]{1,0:T(8,128)} fusion(bf16[1024,2048]{1,0:T(8,128)(2,1)} %all-gather.9.cloned.1.call-done, bf16[2048,1408]{1,0:T(8,128)(2,1)} %all-gather.11.cloned.1.call-done), kind=kOutput, calls=%fused_computation.97 | convolution fusion | flops 5905580032 | bytes 15728640 | tf_op jit(solution)/shard_map/dot_general | solution.py:142
  260.0 7.1 %all-to-all-done.1 = bf16[8,256,1408]{2,1,0:T(8,128)(2,1)} async-done(((bf16[8,256,1408]{2,1,0:T(8,128)(2,1)}), bf16[8,256,1408]{2,1,0:T(8,128)(2,1)}, u32[]{:S(2)}, u32[]{:S(2)}) %all-to-all-start.1) | async-done | bytes 5767200 | tf_op jit(solution)/shard_map/all_to_all | solution.py:150
  267.0 76.3 %all-gather.13.cloned.1.call-done = bf16[1408,2048]{1,0:T(8,128)(2,1)} async-done(((bf16[1408,256]{1,0:T(8,128)(2,1)}), bf16[1408,2048]{1,0:T(8,128)(2,1)}) %all-gather.13.cloned.1.call-update) | async-done | bytes 5767184 | tf_op jit(solution)/shard_map/all_gather | solution.py:154
  343.3 20.5 %convolution_convert_fusion = bf16[1024,2048]{1,0:T(8,128)(2,1)} fusion(bf16[1408,2048]{1,0:T(8,128)(2,1)} %all-gather.13.cloned.1.call-done, f32[1024,1408]{1,0:T(8,128)} %fusion.52, bf16[1024,2048]{1,0:T(8,128)(2,1)} %all-gather.9.cloned.1.call-done, bf16[2048,1408]{1,0:T(8,128)(2,1)} %bitcast.17), kind=kOutput, calls=%fused_computation.38 | convolution fusion | flops 11821907968 | bytes 25690112 | tf_op jit(solution)/shard_map/dot_general | solution.py:157
  363.9 42.9 %reduce-scatter.2.cloned.1.call-done = bf16[256,2048]{1,0:T(8,128)(2,1)} async-done(((bf16[1024,2048]{1,0:T(8,128)(2,1)}), bf16[256,2048]{1,0:T(8,128)(2,1)}) %reduce-scatter.2.cloned.1.call-update) | async-done | bytes 1048592 | tf_op jit(solution)/shard_map/reduce_scatter | solution.py:156
  406.8 1.5 fusion.29
  408.3 2.6 fusion.34
  (74 shorter events, 2.8 us)
Async XLA Ops:
  6.5 25.8 %copy-start.6 = (bf16[1024,256]{1,0:T(8,128)(2,1)S(1)}, bf16[1024,256]{1,0:T(8,128)(2,1)}, u32[]{:S(2)}) copy-start(bf16[1024,256]{1,0:T(8,128)(2,1)} %param.19) | copy-start | bytes 1572868
  6.5 26.0 %copy-start.7 = (bf16[1024,256]{1,0:T(8,128)(2,1)S(1)}, bf16[1024,256]{1,0:T(8,128)(2,1)}, u32[]{:S(2)}) copy-start(bf16[1024,256]{1,0:T(8,128)(2,1)} %param.20) | copy-start | bytes 1572868
  6.5 26.1 %copy-start.1 = (bf16[1024,256]{1,0:T(8,128)(2,1)S(1)}, bf16[1024,256]{1,0:T(8,128)(2,1)}, u32[]{:S(2)}) copy-start(bf16[1024,256]{1,0:T(8,128)(2,1)} %param.18) | copy-start | bytes 1572868
  6.5 84.9 %all-gather.7.cloned.1.call-start = ((), (), s32[]{:S(2)}) async-start(), calls=%async_computation.3 | async-start | bytes 5242880 | tf_op jit(solution)/shard_map/all_gather | solution.py:127
  7.3 25.5 %copy-start.8 = (f32[1024,2]{0,1:T(2,128)S(1)}, f32[1024,2]{0,1:T(2,128)}, u32[]{:S(2)}) copy-start(f32[1024,2]{0,1:T(2,128)} %param.22) | copy-start | bytes 24580
  7.3 177.7 %all-gather.11.cloned.1.call-start = ((), (), s32[]{:S(2)}) async-start(), calls=%async_computation.5 | async-start | bytes 6488064 | tf_op jit(solution)/shard_map/all_gather | solution.py:144
  8.0 240.2 %all-gather.9.cloned.1.call-start = ((), (), s32[]{:S(2)}) async-start(), calls=%async_computation.4 | async-start | bytes 5242880 | tf_op jit(solution)/shard_map/all_gather | solution.py:140
  42.3 2.6 copy-start.5
  44.9 33.4 %copy-start.2 = (bf16[1024,256]{1,0:T(8,128)(2,1)S(1)}, bf16[1024,256]{1,0:T(8,128)(2,1)}, u32[]{:S(2)}) copy-start(bf16[1024,256]{1,0:T(8,128)(2,1)} %param.18) | copy-start | bytes 1572868
  78.3 0.9 copy-start.12
  91.4 3.5 copy-start
  95.4 1.2 copy-start.3
  95.4 1.2 copy-start.9
  96.2 1.1 copy-start.10
  97.3 1.3 copy-start.4
  101.6 165.4 %all-to-all-start.1 = ((bf16[8,256,1408]{2,1,0:T(8,128)(2,1)}), bf16[8,256,1408]{2,1,0:T(8,128)(2,1)}, u32[]{:S(2)}, u32[]{:S(2)}) async-start(bf16[8,256,1408]{2,1,0:T(8,128)(2,1)} %stack.2), calls=%async_computation.1 | async-start | bytes 11534336 | tf_op jit(solution)/shard_map/all_to_all | solution.py:150
  106.3 237.0 %all-gather.13.cloned.1.call-start = ((), (), s32[]{:S(2)}) async-start(), calls=%async_computation.6 | async-start | bytes 6488064 | tf_op jit(solution)/shard_map/all_gather | solution.py:154
  106.9 299.9 %reduce-scatter.2.cloned.1.call-start = ((), (), s32[]{:S(2)}) async-start(), calls=%async_computation.7 | async-start | bytes 5242880 | tf_op jit(solution)/shard_map/reduce_scatter | solution.py:156
  363.8 44.5 %copy-start.11 = (f32[2048]{0:T(1024)S(1)}, f32[2048]{0:T(1024)}, u32[]{:S(2)}) copy-start(f32[2048]{0:T(1024)} %param.31) | copy-start | bytes 24580
Sparse Core Ops, SparseCore 0:
  8.9 37.1 all-gather.6
  48.3 136.6 all-gather.10
  186.6 61.6 all-gather.8
  250.1 93.1 all-gather.12
  364.0 42.7 reduce-scatter.1
